TPU v7x, 32 devices: a whole 2x2x4 slice. The times are simulated.
32 devices in a mesh: sp: 8 (over z, x), tp: 4 (over y, core).
Axes of the slice: x: 2, y: 2, z: 4, core: 2. Of those that a mesh axis runs over, the one named last changes fastest.
Arguments:
- queries: bfloat16 [1024, 2048], P('sp', 'tp'), may hold values from -15 to 15
- key_rows: bfloat16 [1024, 2048], P('sp', 'tp'), may hold values from -6 to 6
- value_rows: bfloat16 [1024, 2048], P('sp', 'tp'), may hold values from -6 to 6
- break_bias: bfloat16 [1024, 16], P('sp', 'tp'), may hold values from -14 to 1
- stream: bfloat16 [1024, 4096], P('sp', 'tp'), may hold values from -24 to 24
- out_proj: bfloat16 [2048, 4096], P(None, 'tp'), may hold values from -0.5 to 0.5
- norm_gain: float32 [4096], P('tp'), may hold values from 0.1 to 1.9
- expert_ids: int32 [1024, 2], P('sp'), may hold values from 0 to 15, all different within a row; in each aligned block of 128 rows (0 to 127, 128 to 255, ...) at most 32 rows name the same one
- route_weights: float32 [1024, 2], P('sp'), may hold values from 0.1 to 2.5
- gate_proj: bfloat16 [16, 4096, 384], P('sp', 'tp'), may hold values from -0.09375 to 0.09375
- up_proj: bfloat16 [16, 4096, 384], P('sp', 'tp'), may hold values from -0.09375 to 0.09375
- down_proj: bfloat16 [16, 384, 4096], P('sp', None, 'tp'), may hold values from -0.3125 to 0.3125
- shared_gate: bfloat16 [4096, 384], P('tp'), may hold values from -0.09375 to 0.09375
- shared_up: bfloat16 [4096, 384], P('tp'), may hold values from -0.09375 to 0.09375
- shared_down: bfloat16 [384, 4096], P(None, 'tp'), may hold values from -0.3125 to 0.3125
Outputs:
- result: bfloat16 [1024, 4096], P('sp', 'tp')
Inputs may be any that keep to these rules, and one draw needn't show every extreme that they name: `expert_ids`: each row names 2 different experts; within the rows of one index of sp no expert is named by more than 32 rows, a bound that some block reaches of them.
All inputs are finite; a program needn't handle non-finite values.
Results may differ from a plain program's by a relative error of at most 0.022.
Values may be sent and summed in bfloat16 or wider, within the bound.
A program may use at most 64 MiB of HBM per device.

v0:
```python
import jax
import jax.numpy as jnp
from jax import lax
from jax.sharding import PartitionSpec as P

D = 4096


EPS = 1e-06
row_block_size = 32


def block_terms(query_heads, key_piece, value_piece, bias_piece, query_pos):
    heads_local = query_heads.shape[1]
    head_dim = query_heads.shape[2]
    key_count = key_piece.shape[0]
    key_heads = key_piece.reshape(key_count, heads_local, head_dim)
    value_heads = value_piece.reshape(key_count, heads_local, head_dim).astype(jnp.float32)
    logits = jnp.einsum("thd,shd->hts", query_heads, key_heads, preferred_element_type=jnp.float32)
    logits = logits * head_dim ** (-0.5) + bias_piece.astype(jnp.float32).T[:, None, :]
    key_pos = jnp.arange(key_count, dtype=jnp.int32)
    before = (key_pos[None, :] < query_pos[:, None])[None]
    log_fail = jnp.where(before, jax.nn.log_sigmoid(-logits), 0.0)
    tail_sum = lax.cumsum(log_fail, axis=2, reverse=True) - log_fail
    weights = jnp.where(before, jnp.exp(jax.nn.log_sigmoid(logits) + tail_sum), 0.0)
    summary = jnp.einsum("hts,shd->thd", weights, value_heads)
    return (summary, jnp.sum(log_fail, axis=2).T)


def body(
    queries,
    key_rows,
    value_rows,
    break_bias,
    stream,
    out_proj,
    norm_gain,
    expert_ids,
    route_weights,
    gate_proj,
    up_proj,
    down_proj,
    shared_gate,
    shared_up,
    shared_down,
):
    tok_dev = queries.shape[0]
    heads_local = break_bias.shape[1]
    head_dim = queries.shape[1] // heads_local
    blocks_all = lax.axis_size("sp")
    own_block = lax.axis_index("sp")
    own_start = own_block * tok_dev
    query_pos = own_start + jnp.arange(tok_dev, dtype=jnp.int32)
    query_heads = queries.reshape(tok_dev, heads_local, head_dim)
    row_step = min(row_block_size, tok_dev)
    row_turns = tok_dev // row_step
    empty_sums = jnp.zeros((blocks_all, tok_dev, heads_local, head_dim), jnp.float32)
    empty_fails = jnp.zeros((blocks_all, tok_dev, heads_local), jnp.float32)
    offset = jnp.int32(0)
    key_piece = lax.all_gather(key_rows, "sp", axis=0, tiled=True)
    value_piece = lax.all_gather(value_rows, "sp", axis=0, tiled=True)
    bias_piece = lax.all_gather(break_bias, "sp", axis=0, tiled=True)
    block_id = offset // tok_dev

    def compute(operand):

        def rows_part(turn):
            row_start = turn * row_step
            part_q = lax.dynamic_slice_in_dim(query_heads, row_start, row_step, 0)
            part_pos = lax.dynamic_slice_in_dim(query_pos, row_start, row_step, 0)
            return block_terms(part_q, key_piece, value_piece, bias_piece, part_pos)

        summary, fail_sum = lax.map(rows_part, jnp.arange(row_turns, dtype=jnp.int32))
        return (
            summary.reshape(tok_dev, heads_local, head_dim),
            fail_sum.reshape(tok_dev, heads_local),
        )

    def skip(operand):
        return (
            jnp.zeros((tok_dev, heads_local, head_dim), jnp.float32),
            jnp.zeros((tok_dev, heads_local), jnp.float32),
        )

    summary, fail_sum = lax.cond(offset < own_start + tok_dev, compute, skip, 0)
    sums_in = empty_sums
    fails_in = empty_fails
    sums_in = lax.dynamic_update_index_in_dim(sums_in, summary, block_id, 0)
    fails_in = lax.dynamic_update_index_in_dim(fails_in, fail_sum, block_id, 0)
    later_fail = jnp.cumsum(fails_in[::-1], axis=0)[::-1] - fails_in
    attended = jnp.sum(jnp.exp(later_fail)[..., None] * sums_in, axis=0)
    attended = attended.reshape(tok_dev, heads_local * head_dim).astype(jnp.bfloat16)
    projected = jnp.dot(
        lax.all_gather(attended, "tp", axis=1, tiled=True),
        out_proj,
        preferred_element_type=jnp.float32,
    )
    mixed = (stream.astype(jnp.float32) + projected).astype(jnp.bfloat16)
    mixed = lax.optimization_barrier(mixed)
    mixed_f = mixed.astype(jnp.float32)
    square_sum = lax.psum(jnp.sum(mixed_f * mixed_f, axis=1), "tp")
    inv_rms = lax.rsqrt(square_sum / D + EPS)
    normed = (mixed_f * inv_rms[:, None] * norm_gain[None, :]).astype(jnp.bfloat16)
    experts_local = gate_proj.shape[0]
    experts_all = experts_local * blocks_all
    top_k = expert_ids.shape[1]
    capacity = 2 * top_k * tok_dev // experts_all
    flat_ids = expert_ids.reshape(-1)
    one_hot = (flat_ids[:, None] == jnp.arange(experts_all, dtype=jnp.int32)[None, :]).astype(
        jnp.int32
    )
    ranks = jnp.sum((jnp.cumsum(one_hot, axis=0) - one_hot) * one_hot, axis=1)
    owner = flat_ids // experts_local
    local_id = flat_ids % experts_local
    slot_index = local_id * (blocks_all * capacity) + owner * capacity + ranks
    token_index = jnp.arange(tok_dev * top_k, dtype=jnp.int32) // top_k
    token_of_slot = (
        jnp.full((experts_all * capacity,), tok_dev, jnp.int32).at[slot_index].set(token_index)
    )
    padded_rows = jnp.concatenate([normed, jnp.zeros((1, normed.shape[1]), jnp.bfloat16)], 0)
    send_rows = padded_rows[token_of_slot].reshape(
        experts_local, blocks_all * capacity, normed.shape[1]
    )
    arrived = lax.all_to_all(send_rows, "sp", split_axis=1, concat_axis=1, tiled=True)
    gate_part = jnp.einsum("erd,edf->erf", arrived, gate_proj, preferred_element_type=jnp.float32)
    up_part = jnp.einsum("erd,edf->erf", arrived, up_proj, preferred_element_type=jnp.float32)
    routed_rows = experts_local * blocks_all * capacity
    gate_part = gate_part.reshape(routed_rows, -1)
    up_part = up_part.reshape(routed_rows, -1)
    shared_gate_part = jnp.dot(normed, shared_gate, preferred_element_type=jnp.float32)
    shared_up_part = jnp.dot(normed, shared_up, preferred_element_type=jnp.float32)
    gate_sum, up_sum, sgate_sum, sup_sum = (
        lax.psum(gate_part.astype(jnp.bfloat16), "tp").astype(jnp.float32),
        lax.psum(up_part.astype(jnp.bfloat16), "tp").astype(jnp.float32),
        lax.psum(shared_gate_part.astype(jnp.bfloat16), "tp").astype(jnp.float32),
        lax.psum(shared_up_part.astype(jnp.bfloat16), "tp").astype(jnp.float32),
    )
    hidden = (jax.nn.silu(gate_sum) * up_sum).astype(jnp.bfloat16)
    shared_hidden = (jax.nn.silu(sgate_sum) * sup_sum).astype(jnp.bfloat16)
    hidden = hidden.reshape(experts_local, blocks_all * capacity, -1)
    expert_out = jnp.einsum(
        "erf,efd->erd", hidden, down_proj, preferred_element_type=jnp.float32
    ).astype(jnp.bfloat16)
    returned = lax.all_to_all(expert_out, "sp", split_axis=1, concat_axis=1, tiled=True)
    flat_back = returned.reshape(experts_all * capacity, -1)
    picked = flat_back[slot_index.reshape(tok_dev, top_k)]
    routed = jnp.einsum("tk,tkd->td", route_weights, picked.astype(jnp.float32))
    shared_out = jnp.dot(shared_hidden, shared_down, preferred_element_type=jnp.float32)
    return (mixed_f + shared_out + routed).astype(jnp.bfloat16)


def solution(mesh):
    in_specs = (
        P("sp", "tp"),
        P("sp", "tp"),
        P("sp", "tp"),
        P("sp", "tp"),
        P("sp", "tp"),
        P(None, "tp"),
        P("tp"),
        P("sp", None),
        P("sp", None),
        P("sp", "tp", None),
        P("sp", "tp", None),
        P("sp", None, "tp"),
        P("tp", None),
        P("tp", None),
        P(None, "tp"),
    )
    out_specs = P("sp", "tp")
    return jax.shard_map(body, mesh=mesh, in_specs=in_specs, out_specs=out_specs, check_vma=False)
```

profile of v0, /device:TPU:0, one launch (start us, length us, event | category | flops | bytes accessed | tf_op | source)
XLA Modules:
  0.0 900.8 jit_solution(6103857424751520015)
XLA Ops:
  11.6 22.5 %all_gather.13 = bf16[1024,4]{0,1:T(4,128)(2,1)S(1)} all-gather(bf16[128,4]{0,1:T(4,128)(2,1)} %param.22), channel_id=1, replica_groups=mesh['sp'=8,'tp'=4] {'sp'}, dimensions={0}, use_global_device_ids=true | all-gather | bytes 9216 | tf_op jit(solution)/shard_map/all_gather | solution.py:62
  34.1 18.3 %all-gather.3.cloned.1.call-done = bf16[1024,512]{1,0:T(8,128)(2,1)} async-done(((bf16[128,512]{1,0:T(8,128)(2,1)}), bf16[1024,512]{1,0:T(8,128)(2,1)}) %all-gather.3.cloned.1.call-update) | async-done | bytes 1048592 | tf_op jit(solution)/shard_map/all_gather | solution.py:60
  52.5 41.1 %all-gather.5.cloned.1.call-done = bf16[1024,512]{1,0:T(8,128)(2,1)} async-done(((bf16[128,512]{1,0:T(8,128)(2,1)}), bf16[1024,512]{1,0:T(8,128)(2,1)}) %all-gather.5.cloned.1.call-update) | async-done | bytes 1048592 | tf_op jit(solution)/shard_map/all_gather | solution.py:61
  93.6 668.0 %conditional.1 = (f32[8,128,4,128]{3,2,1,0:T(4,128)}, f32[8,128,4]{2,1,0:T(8,128)}) conditional(s32[]{:T(128)} %convert_element_type.80, () %tuple.25, (bf16[128,512]{1,0:T(8,128)(2,1)}, s32[]{:T(128)}, s32[128]{0:T(128)S(1)}, bf16[1024,512]{1,0:T(8,128)(2,1)}, bf16[1024,4]{0,1:T(4,128)(2,1)S(1)}, /*index=5*/bf16[1024,512]{1,0:T(8,128)(2,1)}) %tuple.26), branch_computations={%region_0.1_spmd, %region_1.7_spmd} | conditional | flops 89272192 | bytes 12330231 | solution.py:85
  95.4 662.7 %while.11 = (s32[]{:T(128)}, f32[4,32,4,128]{3,2,1,0:T(4,128)}, f32[4,32,4]{1,2,0:T(4,128)S(1)}, s32[4]{0:T(128)S(1)}, s32[128]{0:T(128)S(1)}, /*index=5*/bf16[1...) while((s32[]{:T(128)}, f32[4,32,4,128]{3,2,1,0:T(4,128)}, ...), condition=%wide.region_6.6_spmd, body=%wide.region_2.5_spmd.sunk | while | flops 89272064 | bytes 9422931 | solution.py:73
  96.7 1.7 fusion.91
  99.1 158.4 %reduce-window.24 = f32[4,32,8,128]{3,2,1,0:T(8,128)S(1)} reduce-window(f32[4,32,8,128]{3,2,1,0:T(8,128)S(1)} %bitcast.111, f32[]{:T(128)} %constant.126.clone..sunk), window={size=1x1x1x128 pad=0_0x0_0x0_0x0_127}, to_apply=%region_3.2 | reduce-window | flops 16646144 | bytes 1048580 | tf_op jit(solution)/shard_map/reduce-window
  258.3 2.1 convolution_bitcast_fusion.2
  262.3 1.7 fusion.91
  264.8 158.4 %reduce-window.24 = f32[4,32,8,128]{3,2,1,0:T(8,128)S(1)} reduce-window(f32[4,32,8,128]{3,2,1,0:T(8,128)S(1)} %bitcast.111, f32[]{:T(128)} %constant.126.clone..sunk), window={size=1x1x1x128 pad=0_0x0_0x0_0x0_127}, to_apply=%region_3.2 | reduce-window | flops 16646144 | bytes 1048580 | tf_op jit(solution)/shard_map/reduce-window
  423.9 2.1 convolution_bitcast_fusion.2
  428.0 1.7 fusion.91
  430.5 158.4 %reduce-window.24 = f32[4,32,8,128]{3,2,1,0:T(8,128)S(1)} reduce-window(f32[4,32,8,128]{3,2,1,0:T(8,128)S(1)} %bitcast.111, f32[]{:T(128)} %constant.126.clone..sunk), window={size=1x1x1x128 pad=0_0x0_0x0_0x0_127}, to_apply=%region_3.2 | reduce-window | flops 16646144 | bytes 1048580 | tf_op jit(solution)/shard_map/reduce-window
  589.6 2.1 convolution_bitcast_fusion.2
  593.6 1.7 fusion.91
  596.1 158.4 %reduce-window.24 = f32[4,32,8,128]{3,2,1,0:T(8,128)S(1)} reduce-window(f32[4,32,8,128]{3,2,1,0:T(8,128)S(1)} %bitcast.111, f32[]{:T(128)} %constant.126.clone..sunk), window={size=1x1x1x128 pad=0_0x0_0x0_0x0_127}, to_apply=%region_3.2 | reduce-window | flops 16646144 | bytes 1048580 | tf_op jit(solution)/shard_map/reduce-window
  755.3 2.1 convolution_bitcast_fusion.2
  758.1 2.6 dynamic_update_slice.18
  764.4 2.8 multiply_reduce_fusion
  767.2 7.2 all_gather.15
  775.3 6.4 psum.35
  781.9 2.1 gather_fusion
  783.9 2.1 copy.52
  786.0 3.6 all-to-all-start
  789.8 2.1 convolution_convert_fusion.3
  791.9 2.1 convolution_convert_fusion.4
  793.9 21.1 %all-to-all-done = bf16[2,256,1024]{2,0,1:T(2,128)(2,1)S(1)} async-done(((bf16[2,256,1024]{2,0,1:T(2,128)(2,1)}), bf16[2,256,1024]{2,0,1:T(2,128)(2,1)S(1)}, u32[]{:S(2)}, u32[]{:S(2)}) %all-to-all-start) | async-done | bytes 1048608 | tf_op jit(solution)/shard_map/all_to_all | solution.py:124
  815.0 3.0 convolution_convert_fusion.2
  819.5 34.3 %all-reduce.6.cloned.1.call-done = (bf16[512,384]{1,0:T(8,128)(2,1)}, bf16[512,384]{1,0:T(8,128)(2,1)}, bf16[128,384]{1,0:T(8,128)(2,1)}, bf16[128,384]{1,0:T(8,128)(2,1)}) async-done(((bf16[512,384]{1,0:T(8,128)(2,1)}, bf16[512,384]{1,0:T(8,128)(2,1)}, bf16[128,384]{1,0:T(8,128)(2,1)}, bf16[128,384]{1,0:T(8,128)(2,1)}), (bf16[512,384]{1,0:T(8,128)(2,1)}, bf16[512,384]{1,0:T(8,128)(2,1)}, ...) | async-done | bytes 983056 | tf_op jit(solution)/shard_map/psum | solution.py:134
  855.9 2.1 copy.55
  858.0 5.6 all-to-all-start.1
  864.4 24.8 %all-to-all-done.1 = bf16[2,256,1024]{2,0,1:T(2,128)(2,1)} async-done(((bf16[2,256,1024]{2,0,1:T(2,128)(2,1)}), bf16[2,256,1024]{2,0,1:T(2,128)(2,1)}, u32[]{:S(2)}, u32[]{:S(2)}) %all-to-all-start.1) | async-done | bytes 1048608 | tf_op jit(solution)/shard_map/all_to_all | solution.py:144
  (130 shorter events, 31.9 us)
Async XLA Ops:
  6.5 848.6 %copy-start = (bf16[2,384,1024]{2,1,0:T(8,128)(2,1)S(1)}, bf16[2,384,1024]{2,1,0:T(8,128)(2,1)}, u32[]{:S(2)}) copy-start(bf16[2,384,1024]{2,1,0:T(8,128)(2,1)} %param.30) | copy-start | bytes 4718596
  6.5 45.9 %all-gather.3.cloned.1.call-start = ((), (), s32[]{:S(2)}) async-start(), calls=%async_computation.2 | async-start | bytes 1179648 | tf_op jit(solution)/shard_map/all_gather | solution.py:60
  7.3 86.4 %all-gather.5.cloned.1.call-start = ((), (), s32[]{:S(2)}) async-start(), calls=%async_computation.3 | async-start | bytes 1179648 | tf_op jit(solution)/shard_map/all_gather | solution.py:61
  763.1 11.3 %copy-start.1 = (bf16[2048,1024]{1,0:T(8,128)(2,1)S(1)}, bf16[2048,1024]{1,0:T(8,128)(2,1)}, u32[]{:S(2)}) copy-start(bf16[2048,1024]{1,0:T(8,128)(2,1)} %param.24) | copy-start | bytes 12582916
  764.4 10.0 %copy-start.2 = (bf16[128,1024]{1,0:T(8,128)(2,1)S(1)}, bf16[128,1024]{1,0:T(8,128)(2,1)}, u32[]{:S(2)}) copy-start(bf16[128,1024]{1,0:T(8,128)(2,1)} %param.23) | copy-start | bytes 786436
  774.4 7.3 copy-start.3
  786.0 29.0 %all-to-all-start = ((bf16[2,256,1024]{2,0,1:T(2,128)(2,1)}), bf16[2,256,1024]{2,0,1:T(2,128)(2,1)S(1)}, u32[]{:S(2)}, u32[]{:S(2)}) async-start(bf16[2,256,1024]{2,0,1:T(2,128)(2,1)} %copy.52), calls=%async_computation | async-start | bytes 2097152 | tf_op jit(solution)/shard_map/all_to_all | solution.py:124
  789.6 64.2 %all-reduce.6.cloned.1.call-start = ((), (), s32[]{:S(2)}) async-start(), calls=%async_computation.4 | async-start | bytes 1966080 | tf_op jit(solution)/shard_map/psum | solution.py:134
  815.0 3.0 copy-start.6
  858.0 5.8 copy-start.4
  858.0 6.2 copy-start.5
  858.0 31.2 %all-to-all-start.1 = ((bf16[2,256,1024]{2,0,1:T(2,128)(2,1)}), bf16[2,256,1024]{2,0,1:T(2,128)(2,1)}, u32[]{:S(2)}, u32[]{:S(2)}) async-start(bf16[2,256,1024]{2,0,1:T(2,128)(2,1)} %copy.55), calls=%async_computation.1 | async-start | bytes 2097152 | tf_op jit(solution)/shard_map/all_to_all | solution.py:144
  892.0 1.1 copy-start.7
  892.1 1.1 copy-start.8
  892.1 1.1 copy-start.9
Sparse Core Ops, SparseCore 0:
  9.5 42.9 all-gather.2
  54.6 38.9 all-gather.4
  819.6 34.1 all-reduce.5
where the time goes:
time: 902 us; the launch traced here: 901 us
  other arithmetic  644 us (71%)
  waiting for transfers between devices  141 us (16%)
  blocking collectives  36.1 us (4%)
  matrix products  27.2 us (3%)
  local copies, waits for them, and re-layouts  26.9 us (3%)
  between operations  13.4 us (1%)
  starting transfers between devices  9.46 us (1%)
    another operation x12, other arithmetic  634 us
    all_gather x1, waiting for transfers between devices, body(): value_piece = lax.all_gather(value_rows, 'sp', axis=0, tiled=True)  41.1 us
    psum x1, waiting for transfers between devices, body(): lax.psum(up_part.astype(jnp.bfloat16), 'tp').astype(jnp.float32)  34.3 us
    all_to_all x1, waiting for transfers between devices, body(): lax.all_to_all(expert_out, 'sp', split_axis=1, concat_axis=1, tiled=True)  24.8 us
    all_gather x1, blocking collectives, body(): bias_piece = lax.all_gather(break_bias, 'sp', axis=0, tiled=True)  22.5 us
    all_to_all x1, waiting for transfers between devices, body(): lax.all_to_all(send_rows, 'sp', split_axis=1, concat_axis=1, tiled=True)  21.1 us
    all_gather x1, waiting for transfers between devices, body(): key_piece = lax.all_gather(key_rows, 'sp', axis=0, tiled=True)  18.3 us
  transfers between devices with their start and end apart: 5, of which 5 were waited for; matrix products, arithmetic and copies ran while one was open for 1% of the time, Pallas kernels for 0%

commit v1 on v0

v1 whole, which is shorter than its diff:
```python
import functools

import jax
import jax.numpy as jnp
from jax import lax
from jax.experimental import pallas as pl
from jax.experimental.pallas import tpu as pltpu
from jax.sharding import PartitionSpec as P

EPS = 1e-06
F32 = jnp.float32
BF16 = jnp.bfloat16


def attention_kernel(heads, hd, q_ref, kvb_ref, o_ref, acc, carry):
    tok = q_ref.shape[0]
    own = lax.axis_index("sp")
    scale = hd ** (-0.5)
    row = lax.broadcasted_iota(jnp.int32, (tok, tok), 0)
    col = lax.broadcasted_iota(jnp.int32, (tok, tok), 1)
    later = (row > col).astype(F32)
    sums = jnp.concatenate([later, jnp.ones((tok, tok), F32)], axis=1).astype(BF16)
    sums = jnp.concatenate([sums, sums], axis=0)
    pick_rows = max(16, heads)
    pick = (
        lax.broadcasted_iota(jnp.int32, (pick_rows, hd), 0)
        == lax.broadcasted_iota(jnp.int32, (pick_rows, hd), 1)
    ).astype(F32).astype(BF16)
    acc[...] = jnp.zeros_like(acc)
    carry[...] = jnp.zeros_like(carry)

    def block(j, diagonal):
        start = pl.multiple_of(j * tok, tok)
        piece = kvb_ref.at[pl.ds(start, tok)]
        bias = lax.dot_general(
            pick,
            piece[:, 2 * heads * hd : (2 * heads + 1) * hd],
            (((1,), (1,)), ((), ())),
            preferred_element_type=F32,
        )
        for h in range(heads):
            cols = slice(h * hd, (h + 1) * hd)
            z = lax.dot_general(
                q_ref[:, cols], piece[:, cols], (((1,), (1,)), ((), ())), preferred_element_type=F32
            )
            z = z * scale + bias[h : h + 1, :]
            low = jnp.log1p(jnp.exp(-jnp.abs(z)))
            fail = -(jnp.maximum(z, 0.0) + low)
            hit = jnp.minimum(z, 0.0) - low
            if diagonal:
                before = col < row
                fail = jnp.where(before, fail, 0.0)
            high = fail.astype(BF16)
            rest = (fail - high.astype(F32)).astype(BF16)
            both = jnp.dot(
                jnp.concatenate([high, rest], axis=1), sums, preferred_element_type=F32
            )
            before_sum = carry[h]
            w = jnp.exp(hit + both[:, :tok] + before_sum)
            if diagonal:
                w = jnp.where(before, w, 0.0)
            carry[h] = before_sum + both[:, tok:]
            acc[:, cols] += jnp.dot(
                w.astype(BF16),
                piece[:, heads * hd + h * hd : heads * hd + (h + 1) * hd],
                preferred_element_type=F32,
            )

    block(own, True)

    def step(i, _):
        block(own - 1 - i, False)
        return 0

    lax.fori_loop(0, own, step, 0)
    o_ref[...] = acc[...].astype(BF16)


def attention(queries, kvb, heads, hd):
    tok = queries.shape[0]
    vmem = pl.BlockSpec(memory_space=pltpu.VMEM)
    return pl.pallas_call(
        functools.partial(attention_kernel, heads, hd),
        out_shape=jax.ShapeDtypeStruct((tok, heads * hd), BF16),
        in_specs=[vmem, vmem],
        out_specs=vmem,
        scratch_shapes=[pltpu.VMEM((tok, heads * hd), F32), pltpu.VMEM((heads, tok, tok), F32)],
        compiler_params=pltpu.CompilerParams(vmem_limit_bytes=48 * 2**20),
        cost_estimate=pl.CostEstimate(flops=2 * 10**9, bytes_accessed=2**22, transcendentals=10**6),
    )(queries, kvb)


def body(
    queries,
    key_rows,
    value_rows,
    break_bias,
    stream,
    out_proj,
    norm_gain,
    expert_ids,
    route_weights,
    gate_proj,
    up_proj,
    down_proj,
    shared_gate,
    shared_up,
    shared_down,
):
    tok = queries.shape[0]
    heads = break_bias.shape[1]
    hd = queries.shape[1] // heads
    n_sp = lax.axis_size("sp")
    n_tp = lax.axis_size("tp")
    width = stream.shape[1] * n_tp
    hidden_width = gate_proj.shape[2]

    bias_wide = jnp.pad(break_bias, ((0, 0), (0, hd - heads)))
    kvb = jnp.concatenate([key_rows, value_rows, bias_wide], axis=1)
    kvb = lax.all_gather(kvb, "sp", axis=0, tiled=True)

    experts_local = gate_proj.shape[0]
    experts = experts_local * n_sp
    top_k = expert_ids.shape[1]
    cap = 2 * top_k * tok // experts
    expert_of = jnp.arange(experts, dtype=jnp.int32)
    named = expert_ids[:, :, None] == expert_of[None, None, :]
    named_any = jnp.any(named, axis=1).astype(BF16)
    token = jnp.arange(tok, dtype=jnp.int32)
    earlier = (token[None, :] < token[:, None]).astype(BF16)
    rank_all = jnp.dot(earlier, named_any, preferred_element_type=F32)
    rank = jnp.sum(jnp.where(named, rank_all[:, None, :], 0.0), axis=2).astype(jnp.int32)
    slot = expert_ids * cap + rank
    slots = experts * cap
    place = jnp.arange(slots, dtype=jnp.int32)
    spot = slot[:, :, None] == place[None, None, :]
    send_pick = jnp.any(spot, axis=1).astype(BF16)
    back_pick = jnp.sum(jnp.where(spot, route_weights[:, :, None], 0.0), axis=1).astype(BF16)

    attended = attention(queries, kvb, heads, hd)
    projected = jnp.dot(
        lax.all_gather(attended, "tp", axis=1, tiled=True), out_proj, preferred_element_type=F32
    )
    mixed = (stream.astype(F32) + projected).astype(BF16)
    mixed = lax.optimization_barrier(mixed)
    mixed_f = mixed.astype(F32)
    square_sum = lax.psum(jnp.sum(mixed_f * mixed_f, axis=1), "tp")
    inv_rms = lax.rsqrt(square_sum / width + EPS)
    normed = (mixed_f * inv_rms[:, None] * norm_gain[None, :]).astype(BF16)

    send = lax.dot_general(
        send_pick, normed, (((0,), (0,)), ((), ())), preferred_element_type=F32
    ).astype(BF16)
    send = send.reshape(n_sp, experts_local * cap, normed.shape[1])
    arrived = lax.all_to_all(send, "sp", split_axis=0, concat_axis=0, tiled=True)
    arrived = arrived.reshape(n_sp, experts_local, cap, -1)
    gates, ups = [], []
    for e in range(experts_local):
        rows = arrived[:, e].reshape(n_sp * cap, -1)
        gates.append(jnp.dot(rows, gate_proj[e], preferred_element_type=F32).astype(BF16))
        ups.append(jnp.dot(rows, up_proj[e], preferred_element_type=F32).astype(BF16))
    gates.append(jnp.dot(normed, shared_gate, preferred_element_type=F32).astype(BF16))
    ups.append(jnp.dot(normed, shared_up, preferred_element_type=F32).astype(BF16))
    gate_all = jnp.concatenate(gates, axis=0)
    up_all = jnp.concatenate(ups, axis=0)
    gate_up = jnp.concatenate([gate_all, up_all], axis=1)
    rows_all = gate_up.shape[0]
    parts = lax.all_to_all(
        gate_up.reshape(n_tp, rows_all // n_tp, 2 * hidden_width), "tp", 0, 0, tiled=True
    )
    total = jnp.sum(parts.astype(F32), axis=0)
    hidden = (jax.nn.silu(total[:, :hidden_width]) * total[:, hidden_width:]).astype(BF16)
    hidden = lax.all_gather(hidden, "tp", axis=0, tiled=True)
    outs = []
    for e in range(experts_local):
        rows = hidden[e * n_sp * cap : (e + 1) * n_sp * cap]
        out = jnp.dot(rows, down_proj[e], preferred_element_type=F32).astype(BF16)
        outs.append(out.reshape(n_sp, 1, cap, -1))
    expert_out = jnp.concatenate(outs, axis=1).reshape(n_sp, experts_local * cap, -1)
    returned = lax.all_to_all(expert_out, "sp", split_axis=0, concat_axis=0, tiled=True)
    returned = returned.reshape(slots, -1)
    shared_out = jnp.dot(
        hidden[experts_local * n_sp * cap :], shared_down, preferred_element_type=F32
    )
    routed = jnp.dot(back_pick, returned, preferred_element_type=F32)
    return (mixed_f + shared_out + routed).astype(BF16)


def solution(mesh):
    in_specs = (
        P("sp", "tp"),
        P("sp", "tp"),
        P("sp", "tp"),
        P("sp", "tp"),
        P("sp", "tp"),
        P(None, "tp"),
        P("tp"),
        P("sp", None),
        P("sp", None),
        P("sp", "tp", None),
        P("sp", "tp", None),
        P("sp", None, "tp"),
        P("tp", None),
        P("tp", None),
        P(None, "tp"),
    )
    return jax.shard_map(body, mesh=mesh, in_specs=in_specs, out_specs=P("sp", "tp"), check_vma=False)
```

time: 902 us -> 187 us (0.21)
  other arithmetic: 644 us -> 5.58 us
  waiting for transfers between devices: 141 us -> 102 us
  local copies, waits for them, and re-layouts: 26.9 us -> 4.88 us
  matrix products: 27.2 us -> 8.19 us
    another operation x17 -> x0, other arithmetic: 636 us -> none
    psum x1 -> x0, waiting for transfers between devices: 34.3 us -> none  [body(): lax.psum(up_part.astype(jnp.bfloat16), 'tp').astype(jnp.float32)]
    dot_general x15 -> x12, matrix products: 26.5 us -> 7.45 us  [the longest x1 1.52 us: body(): lax.dot_general(send_pick, normed, (((0,), (0,)), ((), ())), preferred_el...]
    all_to_all x0 -> x1, blocking collectives: none -> 16.3 us  [body(): lax.all_to_all(gate_up.reshape(n_tp, rows_all // n_tp, 2 * hidden_width),...]
    all_gather x1, blocking collectives: 22.5 us -> 6.52 us  [body(): hidden = lax.all_gather(hidden, 'tp', axis=0, tiled=True)]
    all_gather x2 -> x1, waiting for transfers between devices: 59.5 us -> 52.6 us  [body(): kvb = lax.all_gather(kvb, 'sp', axis=0, tiled=True)]
  transfers between devices with their start and end apart: 5 -> 3, of which waited for: 5 -> 3; matrix products, arithmetic and copies ran while one was open for 1% -> 2% of each run, Pallas kernels for 0% -> 0%
where the time goes in v1:
time: 187 us
  waiting for transfers between devices  102 us (55%)
  blocking collectives  36.6 us (20%)
  starting transfers between devices  14.6 us (8%)
  between operations  13.6 us (7%)
  matrix products  8.19 us (4%)
  other arithmetic  5.58 us (3%)
  local copies, waits for them, and re-layouts  4.88 us (3%)
    all_gather x1, waiting for transfers between devices, body(): kvb = lax.all_gather(kvb, 'sp', axis=0, tiled=True)  52.6 us
    all_to_all x1, waiting for transfers between devices, body(): lax.all_to_all(expert_out, 'sp', split_axis=0, concat_axis=0, tiled=True)  26 us
    all_to_all x1, waiting for transfers between devices, body(): lax.all_to_all(send, 'sp', split_axis=0, concat_axis=0, tiled=True)  23.4 us
    all_to_all x1, blocking collectives, body(): lax.all_to_all(gate_up.reshape(n_tp, rows_all // n_tp, 2 * hidden_width),...  16.3 us
    all_to_all x1, starting transfers between devices, body(): lax.all_to_all(send, 'sp', split_axis=0, concat_axis=0, tiled=True)  11 us
    all_gather x1, blocking collectives, body(): lax.all_gather(attended, 'tp', axis=1, tiled=True)  7.29 us
    psum x1, blocking collectives, body(): square_sum = lax.psum(jnp.sum(mixed_f * mixed_f, axis=1), 'tp')  6.55 us
    all_gather x1, blocking collectives, body(): hidden = lax.all_gather(hidden, 'tp', axis=0, tiled=True)  6.52 us
  transfers between devices with their start and end apart: 3, of which 3 were waited for; matrix products, arithmetic and copies ran while one was open for 2% of the time, Pallas kernels for 0%

profile of v1, /device:TPU:0, one launch (start us, length us, event | category | flops | bytes accessed | tf_op | source)
XLA Modules:
  0.0 186.6 jit_solution(3217887008500503927)
XLA Ops:
  6.5 0.9 copy.28
  7.4 1.7 fusion.19
  9.2 0.7 fusion.26
  10.0 0.7 select_reduce_fusion.1
  10.7 0.7 convert_add_fusion
  11.5 52.6 %all-gather.2.cloned.1.call-done.kvb_ref = bf16[1024,1152]{1,0:T(8,128)(2,1)} async-done(((bf16[128,1152]{1,0:T(8,128)(2,1)}), bf16[1024,1152]{1,0:T(8,128)(2,1)}) %all-gather.2.cloned.1.call-update) | async-done | bytes 2359312 | tf_op jit(solution)/shard_map/all_gather | solution.py:120
  64.1 1.7 copy-done.1
  65.8 0.9 copy-done.2
  66.7 1.2 shard_map.145
  67.8 7.3 %all_gather.10 = bf16[128,2048]{1,0:T(8,128)(2,1)S(1)} all-gather(bf16[128,512]{1,0:T(8,128)(2,1)S(1)} %shard_map.145), channel_id=1, replica_groups=mesh['sp'=8,'tp'=4] {'tp'}, dimensions={1}, use_global_device_ids=true | all-gather | bytes 655360 | tf_op jit(solution)/shard_map/all_gather | solution.py:142
  75.1 0.7 fusion.1
  76.0 6.6 %psum.7 = f32[128]{0:T(128)S(1)} all-reduce(f32[128]{0:T(128)S(1)} %fusion.15), channel_id=1, replica_groups=mesh['sp'=8,'tp'=4] {'tp'}, use_global_device_ids=true, to_apply=%region_4.5 | all-reduce | flops 128 | bytes 1024 | tf_op jit(solution)/shard_map/psum | solution.py:147
  82.6 1.5 convolution_convert_fusion
  84.1 11.0 %all-to-all-start = ((bf16[8,64,1024]{2,1,0:T(8,128)(2,1)}), bf16[8,64,1024]{2,1,0:T(8,128)(2,1)S(1)}, u32[]{:S(2)}, u32[]{:S(2)}) async-start(bf16[8,64,1024]{2,1,0:T(8,128)(2,1)} %bitcast), calls=%async_computation | async-start | bytes 2097152 | tf_op jit(solution)/shard_map/all_to_all | solution.py:155
  95.2 0.4 convolution_convert_fusion.7
  95.5 1.5 convolution_convert_fusion.8
  97.0 23.4 %all-to-all-done = bf16[8,64,1024]{2,1,0:T(8,128)(2,1)S(1)} async-done(((bf16[8,64,1024]{2,1,0:T(8,128)(2,1)}), bf16[8,64,1024]{2,1,0:T(8,128)(2,1)S(1)}, u32[]{:S(2)}, u32[]{:S(2)}) %all-to-all-start) | async-done | bytes 1048608 | tf_op jit(solution)/shard_map/all_to_all | solution.py:155
  120.5 1.3 copy-done.7
  121.8 0.4 convolution_convert_fusion.3
  122.2 0.4 convolution_convert_fusion.4
  122.7 0.4 convolution_convert_fusion.5
  123.1 0.4 convolution_convert_fusion.6
  123.7 16.3 %all_to_all.15 = bf16[4,160,768]{2,1,0:T(8,128)(2,1)S(1)} all-to-all(bf16[4,160,768]{2,1,0:T(8,128)(2,1)S(1)} %bitcast.46), channel_id=1, replica_groups=mesh['sp'=8,'tp'=4] {'tp'}, dimensions={0} | all-to-all | bytes 1966080 | tf_op jit(solution)/shard_map/all_to_all | solution.py:168
  140.2 6.5 %all_gather.11 = bf16[640,384]{1,0:T(8,128)(2,1)S(1)} all-gather(bf16[160,384]{1,0:T(8,128)(2,1)S(1)} %fusion.20), channel_id=1, replica_groups=mesh['sp'=8,'tp'=4] {'tp'}, dimensions={0}, use_global_device_ids=true | all-gather | bytes 614400 | tf_op jit(solution)/shard_map/all_gather | solution.py:173
  146.7 0.4 convolution_convert_fusion.1
  147.1 0.4 convolution_convert_fusion.2
  147.6 1.1 pad_maximum_fusion
  148.7 3.6 %all-to-all-start.2 = ((bf16[8,64,1024]{2,1,0:T(8,128)(2,1)}), bf16[8,64,1024]{2,1,0:T(8,128)(2,1)S(1)}, u32[]{:S(2)}, u32[]{:S(2)}) async-start(bf16[8,64,1024]{2,1,0:T(8,128)(2,1)} %bitcast.15), calls=%async_computation.2 | async-start | bytes 2097152 | tf_op jit(solution)/shard_map/all_to_all | solution.py:180
  152.3 0.1 select_reduce_fusion
  152.4 0.3 convolution_add_fusion.2
  152.7 26.0 %all-to-all-done.2 = bf16[8,64,1024]{2,1,0:T(8,128)(2,1)S(1)} async-done(((bf16[8,64,1024]{2,1,0:T(8,128)(2,1)}), bf16[8,64,1024]{2,1,0:T(8,128)(2,1)S(1)}, u32[]{:S(2)}, u32[]{:S(2)}) %all-to-all-start.2) | async-done | bytes 1048608 | tf_op jit(solution)/shard_map/all_to_all | solution.py:180
  178.7 1.0 fusion
  (29 shorter events, 0.8 us)
Async XLA Ops:
  6.5 145.9 %copy-start = (bf16[384,1024]{1,0:T(8,128)(2,1)S(1)}, bf16[384,1024]{1,0:T(8,128)(2,1)}, u32[]{:S(2)}) copy-start(bf16[384,1024]{1,0:T(8,128)(2,1)} %param.29) | copy-start | bytes 2359300
  6.5 57.5 %all-gather.2.cloned.1.call-start = ((), (), s32[]{:S(2)}) async-start(), calls=%async_computation.3 | async-start | bytes 2654208 | tf_op jit(solution)/shard_map/all_gather | solution.py:120
  64.1 1.7 copy-start.1
  65.8 0.9 copy-start.2
  66.7 8.5 %copy-start.3 = (bf16[2048,1024]{1,0:T(8,128)(2,1)S(1)}, bf16[2048,1024]{1,0:T(8,128)(2,1)}, u32[]{:S(2)}) copy-start(bf16[2048,1024]{1,0:T(8,128)(2,1)} %param.20) | copy-start | bytes 12582916
  66.7 8.5 %copy-start.4 = (bf16[128,1024]{1,0:T(8,128)(2,1)S(1)}, bf16[128,1024]{1,0:T(8,128)(2,1)}, u32[]{:S(2)}) copy-start(bf16[128,1024]{1,0:T(8,128)(2,1)} %param.19) | copy-start | bytes 786436
  75.1 7.5 %copy-start.5 = (f32[1024]{0:T(1024)S(1)}, f32[1024]{0:T(1024)}, u32[]{:S(2)}) copy-start(f32[1024]{0:T(1024)} %param.21) | copy-start | bytes 12292
  75.9 19.3 %copy-start.10 = (bf16[1024,384]{1,0:T(8,128)(2,1)S(1)}, bf16[1024,384]{1,0:T(8,128)(2,1)}, u32[]{:S(2)}) copy-start(bf16[1024,384]{1,0:T(8,128)(2,1)} %param.28) | copy-start | bytes 2359300
  84.1 36.3 %all-to-all-start = ((bf16[8,64,1024]{2,1,0:T(8,128)(2,1)}), bf16[8,64,1024]{2,1,0:T(8,128)(2,1)S(1)}, u32[]{:S(2)}, u32[]{:S(2)}) async-start(bf16[8,64,1024]{2,1,0:T(8,128)(2,1)} %bitcast), calls=%async_computation | async-start | bytes 2097152 | tf_op jit(solution)/shard_map/all_to_all | solution.py:155
  120.4 1.4 copy-start.7
  120.5 2.2 %copy-start.8 = (bf16[2,1024,384]{2,1,0:T(8,128)(2,1)S(1)}, bf16[2,1024,384]{2,1,0:T(8,128)(2,1)}, u32[]{:S(2)}) copy-start(bf16[2,1024,384]{2,1,0:T(8,128)(2,1)} %param.24) | copy-start | bytes 4718596
  123.7 23.0 %copy-start.9 = (bf16[2,384,1024]{2,1,0:T(8,128)(2,1)S(1)}, bf16[2,384,1024]{2,1,0:T(8,128)(2,1)}, u32[]{:S(2)}) copy-start(bf16[2,384,1024]{2,1,0:T(8,128)(2,1)} %param.26) | copy-start | bytes 4718596
  147.6 4.7 %copy-start.6 = (f32[128,2]{0,1:T(2,128)S(1)}, f32[128,2]{0,1:T(2,128)}, u32[]{:S(2)}) copy-start(f32[128,2]{0,1:T(2,128)} %param.23) | copy-start | bytes 3076
  148.7 30.0 %all-to-all-start.2 = ((bf16[8,64,1024]{2,1,0:T(8,128)(2,1)}), bf16[8,64,1024]{2,1,0:T(8,128)(2,1)S(1)}, u32[]{:S(2)}, u32[]{:S(2)}) async-start(bf16[8,64,1024]{2,1,0:T(8,128)(2,1)} %bitcast.15), calls=%async_computation.2 | async-start | bytes 2097152 | tf_op jit(solution)/shard_map/all_to_all | solution.py:180
Sparse Core Ops, SparseCore 0:
  9.5 54.5 all-gather.1

commit v2 on v1

--- a/solution.py
+++ b/solution.py
@@ -12,9 +12,90 @@
 BF16 = jnp.bfloat16
 
 
-def attention_kernel(heads, hd, q_ref, kvb_ref, o_ref, acc, carry):
+def attention_kernel(
+    heads, hd, n_sp, inner, q_ref, k_ref, v_ref, b_ref, o_ref, kbuf, vbuf, bbuf, acc, carry, send_sem, recv_sem
+):
     tok = q_ref.shape[0]
     own = lax.axis_index("sp")
+    outer = n_sp // inner
+    z_own = own // inner
+    x_own = own % inner
+    above = z_own < outer - 1
+    below = z_own > 0
+
+    barrier = pltpu.get_barrier_semaphore()
+
+    def greet(target):
+        pl.semaphore_signal(
+            barrier, inc=1, device_id={"sp": target}, device_id_type=pl.DeviceIdType.MESH
+        )
+
+    @pl.when(above)
+    def _():
+        greet(own + inner)
+
+    @pl.when(below)
+    def _():
+        greet(own - inner)
+
+    for d in range(1, inner):
+        greet(z_own * inner + (x_own + d) % inner)
+    pl.semaphore_wait(barrier, inner - 1 + above.astype(jnp.int32) + below.astype(jnp.int32))
+
+    def copies(sources, block, z_block, lane, target):
+        return [
+            pltpu.make_async_remote_copy(
+                src_ref=src,
+                dst_ref=dst.at[block],
+                send_sem=send_sem.at[kind, z_block, lane],
+                recv_sem=recv_sem.at[kind, block],
+                device_id={"sp": target},
+                device_id_type=pl.DeviceIdType.MESH,
+            )
+            for kind, (src, dst) in enumerate(zip(sources, (kbuf, vbuf, bbuf)))
+        ]
+
+    def held(block):
+        return (kbuf.at[block], vbuf.at[block], bbuf.at[block])
+
+    def start_all(group):
+        for c in group:
+            c.start()
+
+    def wait_sent(group):
+        for c in group:
+            c.wait_send()
+
+    def wait_arrived(block):
+        for c in copies(held(block), block, 0, 0, (own + 1) % n_sp):
+            c.wait_recv()
+
+    def own_sends(act):
+        mine = (k_ref, v_ref, b_ref)
+
+        @pl.when(above)
+        def _():
+            act(copies(mine, own, z_own, 0, own + inner))
+
+        for d in range(1, inner):
+            x_to = (x_own + d) % inner
+
+            @pl.when(x_to > x_own)
+            def _():
+                act(copies(mine, own, z_own, d, z_own * inner + x_to))
+
+    def relays(z_block, act):
+        block = z_block * inner + x_own
+
+        @pl.when(above)
+        def _():
+            act(copies(held(block), block, z_block, 0, own + inner))
+
+        for d in range(1, inner):
+            act(copies(held(block), block, z_block, d, z_own * inner + (x_own + d) % inner))
+
+    own_sends(start_all)
+
     scale = hd ** (-0.5)
     row = lax.broadcasted_iota(jnp.int32, (tok, tok), 0)
     col = lax.broadcasted_iota(jnp.int32, (tok, tok), 1)
@@ -29,19 +110,14 @@
     acc[...] = jnp.zeros_like(acc)
     carry[...] = jnp.zeros_like(carry)
 
-    def block(j, diagonal):
-        start = pl.multiple_of(j * tok, tok)
-        piece = kvb_ref.at[pl.ds(start, tok)]
+    def compute(keys, values, offsets, diagonal):
         bias = lax.dot_general(
-            pick,
-            piece[:, 2 * heads * hd : (2 * heads + 1) * hd],
-            (((1,), (1,)), ((), ())),
-            preferred_element_type=F32,
+            pick, offsets[...], (((1,), (1,)), ((), ())), preferred_element_type=F32
         )
         for h in range(heads):
             cols = slice(h * hd, (h + 1) * hd)
             z = lax.dot_general(
-                q_ref[:, cols], piece[:, cols], (((1,), (1,)), ((), ())), preferred_element_type=F32
+                q_ref[:, cols], keys[:, cols], (((1,), (1,)), ((), ())), preferred_element_type=F32
             )
             z = z * scale + bias[h : h + 1, :]
             low = jnp.log1p(jnp.exp(-jnp.abs(z)))
@@ -60,34 +136,70 @@
             if diagonal:
                 w = jnp.where(before, w, 0.0)
             carry[h] = before_sum + both[:, tok:]
-            acc[:, cols] += jnp.dot(
-                w.astype(BF16),
-                piece[:, heads * hd + h * hd : heads * hd + (h + 1) * hd],
-                preferred_element_type=F32,
-            )
-
-    block(own, True)
-
-    def step(i, _):
-        block(own - 1 - i, False)
+            acc[:, cols] += jnp.dot(w.astype(BF16), values[:, cols], preferred_element_type=F32)
+
+    compute(k_ref, v_ref, b_ref, True)
+
+    def group(i, _):
+        z_block = z_own - i
+
+        @pl.when(z_block > 0)
+        def _():
+            wait_arrived((z_block - 1) * inner + x_own)
+            relays(z_block - 1, start_all)
+
+        def member(m, _):
+            x_block = inner - 1 - m
+            block = z_block * inner + x_block
+
+            @pl.when(block < own)
+            def _():
+                @pl.when(x_block != x_own)
+                def _():
+                    wait_arrived(block)
+
+                compute(*held(block), False)
+
+            return 0
+
+        lax.fori_loop(0, inner, member, 0)
         return 0
 
-    lax.fori_loop(0, own, step, 0)
+    lax.fori_loop(0, z_own + 1, group, 0)
     o_ref[...] = acc[...].astype(BF16)
 
-
-def attention(queries, kvb, heads, hd):
+    own_sends(wait_sent)
+
+    def drain(z_block, _):
+        relays(z_block, wait_sent)
+        return 0
+
+    lax.fori_loop(0, z_own, drain, 0)
+
+
+def attention(queries, keys, values, bias, heads, hd, n_sp):
     tok = queries.shape[0]
+    inner = max(d for d in range(1, n_sp + 1) if n_sp % d == 0 and d * d <= n_sp)
     vmem = pl.BlockSpec(memory_space=pltpu.VMEM)
     return pl.pallas_call(
-        functools.partial(attention_kernel, heads, hd),
+        functools.partial(attention_kernel, heads, hd, n_sp, inner),
         out_shape=jax.ShapeDtypeStruct((tok, heads * hd), BF16),
-        in_specs=[vmem, vmem],
+        in_specs=[vmem] * 4,
         out_specs=vmem,
-        scratch_shapes=[pltpu.VMEM((tok, heads * hd), F32), pltpu.VMEM((heads, tok, tok), F32)],
-        compiler_params=pltpu.CompilerParams(vmem_limit_bytes=48 * 2**20),
+        scratch_shapes=[
+            pltpu.VMEM((n_sp, tok, heads * hd), BF16),
+            pltpu.VMEM((n_sp, tok, heads * hd), BF16),
+            pltpu.VMEM((n_sp, tok, hd), BF16),
+            pltpu.VMEM((tok, heads * hd), F32),
+            pltpu.VMEM((heads, tok, tok), F32),
+            pltpu.SemaphoreType.DMA((3, n_sp // inner, inner)),
+            pltpu.SemaphoreType.DMA((3, n_sp)),
+        ],
+        compiler_params=pltpu.CompilerParams(
+            vmem_limit_bytes=40 * 2**20, collective_id=0, has_side_effects=True
+        ),
         cost_estimate=pl.CostEstimate(flops=2 * 10**9, bytes_accessed=2**22, transcendentals=10**6),
-    )(queries, kvb)
+    )(queries, keys, values, bias)
 
 
 def body(
@@ -116,8 +228,6 @@
     hidden_width = gate_proj.shape[2]
 
     bias_wide = jnp.pad(break_bias, ((0, 0), (0, hd - heads)))
-    kvb = jnp.concatenate([key_rows, value_rows, bias_wide], axis=1)
-    kvb = lax.all_gather(kvb, "sp", axis=0, tiled=True)
 
     experts_local = gate_proj.shape[0]
     experts = experts_local * n_sp
@@ -137,7 +247,7 @@
     send_pick = jnp.any(spot, axis=1).astype(BF16)
     back_pick = jnp.sum(jnp.where(spot, route_weights[:, :, None], 0.0), axis=1).astype(BF16)
 
-    attended = attention(queries, kvb, heads, hd)
+    attended = attention(queries, key_rows, value_rows, bias_wide, heads, hd, n_sp)
     projected = jnp.dot(
         lax.all_gather(attended, "tp", axis=1, tiled=True), out_proj, preferred_element_type=F32
     )

time: 187 us -> 143 us (0.76)
  waiting for transfers between devices: 102 us -> 49.4 us
  starting transfers between devices: 14.6 us -> 32 us
  between operations: 13.6 us -> 0.24 us
  Pallas kernels: 1.17 us -> 9.76 us
  other arithmetic: 5.58 us -> 1.83 us
    all_gather x1 -> x0, waiting for transfers between devices: 52.6 us -> none  [body(): kvb = lax.all_gather(kvb, 'sp', axis=0, tiled=True)]
    all_to_all x1, starting transfers between devices: 11 us -> 28.4 us  [body(): lax.all_to_all(send, 'sp', split_axis=0, concat_axis=0, tiled=True)]
    pallas_call x1, Pallas kernels: 1.17 us -> 9.76 us  [attention(): pl.pallas_call(functools.partial(attention_kernel, heads, hd, n_sp, inner...]
    unnamed x23 -> x27, local copies, waits for them, and re-layouts: 4.81 us -> 4.95 us
  transfers between devices with their start and end apart: 3 -> 2, of which waited for: 3 -> 2; matrix products, arithmetic and copies ran while one was open for 2% -> 2% of each run, Pallas kernels for 0% -> 0%
where the time goes in v2:
time: 143 us
  waiting for transfers between devices  49.4 us (35%)
  blocking collectives  36.5 us (26%)
  starting transfers between devices  32 us (22%)
  Pallas kernels  9.76 us (7%)
  matrix products  8.2 us (6%)
  local copies, waits for them, and re-layouts  5.03 us (4%)
  other arithmetic  1.83 us (1%)
    all_to_all x1, starting transfers between devices, body(): lax.all_to_all(send, 'sp', split_axis=0, concat_axis=0, tiled=True)  28.4 us
    all_to_all x1, waiting for transfers between devices, body(): lax.all_to_all(expert_out, 'sp', split_axis=0, concat_axis=0, tiled=True)  26 us
    all_to_all x1, waiting for transfers between devices, body(): lax.all_to_all(send, 'sp', split_axis=0, concat_axis=0, tiled=True)  23.4 us
    all_to_all x1, blocking collectives, body(): lax.all_to_all(gate_up.reshape(n_tp, rows_all // n_tp, 2 * hidden_width),...  16.3 us
    pallas_call x1, Pallas kernels, attention(): pl.pallas_call(functools.partial(attention_kernel, heads, hd, n_sp, inner...  9.76 us
    all_gather x1, blocking collectives, body(): lax.all_gather(attended, 'tp', axis=1, tiled=True)  7.2 us
    psum x1, blocking collectives, body(): square_sum = lax.psum(jnp.sum(mixed_f * mixed_f, axis=1), 'tp')  6.56 us
    all_gather x1, blocking collectives, body(): hidden = lax.all_gather(hidden, 'tp', axis=0, tiled=True)  6.52 us
  transfers between devices with their start and end apart: 2, of which 2 were waited for; matrix products, arithmetic and copies ran while one was open for 2% of the time, Pallas kernels for 0%

profile of v2, /device:TPU:0, one launch (start us, length us, event | category | flops | bytes accessed | tf_op | source)
XLA Modules:
  0.0 142.9 jit_solution(4164090752778931562)
XLA Ops:
  0.0 0.9 copy.28
  0.9 0.9 copy-done.1
  1.8 0.9 copy-done.2
  2.7 0.9 copy-done.3
  3.6 9.8 %shard_map.145 = bf16[128,512]{1,0:T(8,128)(2,1)S(1)} custom-call(bf16[128,512]{1,0:T(8,128)(2,1)S(1)} %copy-done.1, bf16[128,512]{1,0:T(8,128)(2,1)S(1)} %copy-done.2, bf16[128,512]{1,0:T(8,128)(2,1)S(1)} %copy-done.3, bf16[128,128]{1,0:T(8,128)(2,1)S(1)} %pad.4.b_ref), custom_call_target="tpu_custom_call" | custom-call | flops 2000000000 | bytes 4194304 | tf_op jit(solution)/shard_map/pallas_call | solution.py:184
  13.4 7.2 %all_gather.6 = bf16[128,2048]{1,0:T(8,128)(2,1)S(1)} all-gather(bf16[128,512]{1,0:T(8,128)(2,1)S(1)} %shard_map.145), channel_id=1, replica_groups=mesh['sp'=8,'tp'=4] {'tp'}, dimensions={1}, use_global_device_ids=true | all-gather | bytes 655360 | tf_op jit(solution)/shard_map/all_gather | solution.py:252
  20.6 0.8 fusion.1
  21.4 0.1 fusion.14
  21.5 6.6 %psum.7 = f32[128]{0:T(128)S(1)} all-reduce(f32[128]{0:T(128)S(1)} %fusion.14), channel_id=1, replica_groups=mesh['sp'=8,'tp'=4] {'tp'}, use_global_device_ids=true, to_apply=%region_4.5 | all-reduce | flops 128 | bytes 1024 | tf_op jit(solution)/shard_map/psum | solution.py:257
  28.1 0.1 fusion.23
  28.3 0.1 fusion.17
  28.4 1.5 %convolution_convert_fusion = bf16[512,1024]{1,0:T(8,128)(2,1)} fusion(pred[128,512]{1,0:T(8,128)(4,1)S(1)} %fusion.17, bf16[128,1024]{1,0:T(8,128)(2,1)S(1)} %fusion.1, f32[1024]{0:T(1024)S(1)} %copy-done.7, f32[128]{0:T(128)S(1)} %add_rsqrt_fusion), kind=kOutput, calls=%fused_computation.1 | convolution fusion | flops 135266304 | bytes 1380864 | tf_op jit(solution)/shard_map/dot_general | solution.py:261
  29.9 28.4 %all-to-all-start = ((bf16[8,64,1024]{2,1,0:T(8,128)(2,1)}), bf16[8,64,1024]{2,1,0:T(8,128)(2,1)S(1)}, u32[]{:S(2)}, u32[]{:S(2)}) async-start(bf16[8,64,1024]{2,1,0:T(8,128)(2,1)} %bitcast), calls=%async_computation | async-start | bytes 2097152 | tf_op jit(solution)/shard_map/all_to_all | solution.py:265
  58.3 0.4 convolution_convert_fusion.7
  58.7 1.5 %convolution_convert_fusion.8 = bf16[128,384]{1,0:T(8,128)(2,1)S(1)} fusion(bf16[1024,384]{1,0:T(8,128)(2,1)} %param.27, bf16[128,1024]{1,0:T(8,128)(2,1)S(1)} %fusion.1, f32[1024]{0:T(1024)S(1)} %copy-done.7, f32[128]{0:T(128)S(1)} %add_rsqrt_fusion), kind=kOutput, calls=%fused_computation.14 | convolution fusion | flops 101236736 | bytes 1151488 | tf_op jit(solution)/shard_map/dot_general | solution.py:272
  60.2 23.4 %all-to-all-done = bf16[8,64,1024]{2,1,0:T(8,128)(2,1)S(1)} async-done(((bf16[8,64,1024]{2,1,0:T(8,128)(2,1)}), bf16[8,64,1024]{2,1,0:T(8,128)(2,1)S(1)}, u32[]{:S(2)}, u32[]{:S(2)}) %all-to-all-start) | async-done | bytes 1048608 | tf_op jit(solution)/shard_map/all_to_all | solution.py:265
  83.7 1.3 copy-done.9
  85.0 0.4 convolution_convert_fusion.3
  85.4 0.4 convolution_convert_fusion.4
  85.9 0.4 convolution_convert_fusion.5
  86.3 0.4 convolution_convert_fusion.6
  86.9 16.3 %all_to_all.15 = bf16[4,160,768]{2,1,0:T(8,128)(2,1)S(1)} all-to-all(bf16[4,160,768]{2,1,0:T(8,128)(2,1)S(1)} %bitcast.46), channel_id=1, replica_groups=mesh['sp'=8,'tp'=4] {'tp'}, dimensions={0} | all-to-all | bytes 1966080 | tf_op jit(solution)/shard_map/all_to_all | solution.py:278
  103.1 0.1 convert_reduce_fusion
  103.4 6.5 %all_gather.7 = bf16[640,384]{1,0:T(8,128)(2,1)S(1)} all-gather(bf16[160,384]{1,0:T(8,128)(2,1)S(1)} %fusion.18), channel_id=1, replica_groups=mesh['sp'=8,'tp'=4] {'tp'}, dimensions={0}, use_global_device_ids=true | all-gather | bytes 614400 | tf_op jit(solution)/shard_map/all_gather | solution.py:283
  109.9 0.4 convolution_convert_fusion.1
  110.3 0.4 convolution_convert_fusion.2
  110.8 1.1 pad_maximum_fusion
  111.9 3.6 %all-to-all-start.2 = ((bf16[8,64,1024]{2,1,0:T(8,128)(2,1)}), bf16[8,64,1024]{2,1,0:T(8,128)(2,1)S(1)}, u32[]{:S(2)}, u32[]{:S(2)}) async-start(bf16[8,64,1024]{2,1,0:T(8,128)(2,1)} %bitcast.15), calls=%async_computation.2 | async-start | bytes 2097152 | tf_op jit(solution)/shard_map/all_to_all | solution.py:290
  115.4 0.1 select_reduce_fusion
  115.6 0.3 convolution_add_fusion.2
  115.9 26.0 %all-to-all-done.2 = bf16[8,64,1024]{2,1,0:T(8,128)(2,1)S(1)} async-done(((bf16[8,64,1024]{2,1,0:T(8,128)(2,1)}), bf16[8,64,1024]{2,1,0:T(8,128)(2,1)S(1)}, u32[]{:S(2)}, u32[]{:S(2)}) %all-to-all-start.2) | async-done | bytes 1048608 | tf_op jit(solution)/shard_map/all_to_all | solution.py:290
  141.9 1.0 fusion
  (30 shorter events, 0.3 us)
Async XLA Ops:
  0.0 115.6 %copy-start = (bf16[384,1024]{1,0:T(8,128)(2,1)S(1)}, bf16[384,1024]{1,0:T(8,128)(2,1)}, u32[]{:S(2)}) copy-start(bf16[384,1024]{1,0:T(8,128)(2,1)} %param.29) | copy-start | bytes 2359300
  0.9 0.9 copy-start.1
  1.8 0.9 copy-start.2
  2.7 0.9 copy-start.3
  3.6 17.0 %copy-start.4 = (bf16[2048,1024]{1,0:T(8,128)(2,1)S(1)}, bf16[2048,1024]{1,0:T(8,128)(2,1)}, u32[]{:S(2)}) copy-start(bf16[2048,1024]{1,0:T(8,128)(2,1)} %param.20) | copy-start | bytes 12582916
  3.6 17.0 %copy-start.5 = (bf16[128,1024]{1,0:T(8,128)(2,1)S(1)}, bf16[128,1024]{1,0:T(8,128)(2,1)}, u32[]{:S(2)}) copy-start(bf16[128,1024]{1,0:T(8,128)(2,1)} %param.19) | copy-start | bytes 786436
  20.6 7.5 %copy-start.6 = (s32[128,2]{0,1:T(2,128)S(1)}, s32[128,2]{0,1:T(2,128)}, u32[]{:S(2)}) copy-start(s32[128,2]{0,1:T(2,128)} %param.22) | copy-start | bytes 3076
  20.6 7.8 %copy-start.7 = (f32[1024]{0:T(1024)S(1)}, f32[1024]{0:T(1024)}, u32[]{:S(2)}) copy-start(f32[1024]{0:T(1024)} %param.21) | copy-start | bytes 12292
  21.4 37.0 %copy-start.12 = (bf16[1024,384]{1,0:T(8,128)(2,1)S(1)}, bf16[1024,384]{1,0:T(8,128)(2,1)}, u32[]{:S(2)}) copy-start(bf16[1024,384]{1,0:T(8,128)(2,1)} %param.28) | copy-start | bytes 2359300
  29.9 53.6 %all-to-all-start = ((bf16[8,64,1024]{2,1,0:T(8,128)(2,1)}), bf16[8,64,1024]{2,1,0:T(8,128)(2,1)S(1)}, u32[]{:S(2)}, u32[]{:S(2)}) async-start(bf16[8,64,1024]{2,1,0:T(8,128)(2,1)} %bitcast), calls=%async_computation | async-start | bytes 2097152 | tf_op jit(solution)/shard_map/all_to_all | solution.py:265
  83.6 1.4 copy-start.9
  83.7 2.2 %copy-start.10 = (bf16[2,1024,384]{2,1,0:T(8,128)(2,1)S(1)}, bf16[2,1024,384]{2,1,0:T(8,128)(2,1)}, u32[]{:S(2)}) copy-start(bf16[2,1024,384]{2,1,0:T(8,128)(2,1)} %param.24) | copy-start | bytes 4718596
  86.9 23.0 %copy-start.11 = (bf16[2,384,1024]{2,1,0:T(8,128)(2,1)S(1)}, bf16[2,384,1024]{2,1,0:T(8,128)(2,1)}, u32[]{:S(2)}) copy-start(bf16[2,384,1024]{2,1,0:T(8,128)(2,1)} %param.26) | copy-start | bytes 4718596
  110.8 4.7 %copy-start.8 = (f32[128,2]{0,1:T(2,128)S(1)}, f32[128,2]{0,1:T(2,128)}, u32[]{:S(2)}) copy-start(f32[128,2]{0,1:T(2,128)} %param.23) | copy-start | bytes 3076
  111.9 30.0 %all-to-all-start.2 = ((bf16[8,64,1024]{2,1,0:T(8,128)(2,1)}), bf16[8,64,1024]{2,1,0:T(8,128)(2,1)S(1)}, u32[]{:S(2)}, u32[]{:S(2)}) async-start(bf16[8,64,1024]{2,1,0:T(8,128)(2,1)} %bitcast.15), calls=%async_computation.2 | async-start | bytes 2097152 | tf_op jit(solution)/shard_map/all_to_all | solution.py:290

commit v3 on v2

--- a/solution.py
+++ b/solution.py
@@ -202,6 +202,79 @@
     )(queries, keys, values, bias)
 
 
+def exchange_kernel(n_tp, gu_ref, o_ref, parts, mine, spread, send_parts, recv_parts, send_rows, recv_rows):
+    width = gu_ref.shape[2] // 2
+    me = lax.axis_index("tp")
+    barrier = pltpu.get_barrier_semaphore()
+    others = [(me + d) % n_tp for d in range(1, n_tp)]
+    for to in others:
+        pl.semaphore_signal(
+            barrier, inc=1, device_id={"tp": to}, device_id_type=pl.DeviceIdType.MESH
+        )
+    pl.semaphore_wait(barrier, n_tp - 1)
+    first, second = [], []
+    for d, to in enumerate(others):
+        copy = pltpu.make_async_remote_copy(
+            src_ref=gu_ref.at[to],
+            dst_ref=parts.at[d],
+            send_sem=send_parts.at[d],
+            recv_sem=recv_parts.at[d],
+            device_id={"tp": to},
+            device_id_type=pl.DeviceIdType.MESH,
+        )
+        copy.start()
+        first.append(copy)
+    total = gu_ref[me].astype(F32)
+    for d, copy in enumerate(first):
+        copy.wait_recv()
+        total = total + parts[d].astype(F32)
+    gate = total[:, :width]
+    mine[...] = (jax.nn.silu(gate) * total[:, width:]).astype(BF16)
+    for d, to in enumerate(others):
+        copy = pltpu.make_async_remote_copy(
+            src_ref=mine,
+            dst_ref=spread.at[d],
+            send_sem=send_rows.at[d],
+            recv_sem=recv_rows.at[d],
+            device_id={"tp": to},
+            device_id_type=pl.DeviceIdType.MESH,
+        )
+        copy.start()
+        second.append(copy)
+    o_ref[me] = mine[...]
+    for d, copy in enumerate(second):
+        copy.wait_recv()
+        o_ref[(me + n_tp - 1 - d) % n_tp] = spread[d]
+    for copy in first + second:
+        copy.wait_send()
+
+
+def exchange(gate_up, n_tp):
+    rows, width = gate_up.shape[0] // n_tp, gate_up.shape[1] // 2
+    vmem = pl.BlockSpec(memory_space=pltpu.VMEM)
+    dma = pltpu.SemaphoreType.DMA((n_tp - 1,))
+    hidden = pl.pallas_call(
+        functools.partial(exchange_kernel, n_tp),
+        out_shape=jax.ShapeDtypeStruct((n_tp, rows, width), BF16),
+        in_specs=[vmem],
+        out_specs=vmem,
+        scratch_shapes=[
+            pltpu.VMEM((n_tp - 1, rows, 2 * width), BF16),
+            pltpu.VMEM((rows, width), BF16),
+            pltpu.VMEM((n_tp - 1, rows, width), BF16),
+            dma,
+            dma,
+            dma,
+            dma,
+        ],
+        compiler_params=pltpu.CompilerParams(
+            vmem_limit_bytes=24 * 2**20, collective_id=1, has_side_effects=True
+        ),
+        cost_estimate=pl.CostEstimate(flops=10**8, bytes_accessed=2**21, transcendentals=10**5),
+    )(gate_up.reshape(n_tp, rows, 2 * width))
+    return hidden.reshape(n_tp * rows, width)
+
+
 def body(
     queries,
     key_rows,
@@ -225,7 +298,6 @@
     n_sp = lax.axis_size("sp")
     n_tp = lax.axis_size("tp")
     width = stream.shape[1] * n_tp
-    hidden_width = gate_proj.shape[2]
 
     bias_wide = jnp.pad(break_bias, ((0, 0), (0, hd - heads)))
 
@@ -274,13 +346,7 @@
     gate_all = jnp.concatenate(gates, axis=0)
     up_all = jnp.concatenate(ups, axis=0)
     gate_up = jnp.concatenate([gate_all, up_all], axis=1)
-    rows_all = gate_up.shape[0]
-    parts = lax.all_to_all(
-        gate_up.reshape(n_tp, rows_all // n_tp, 2 * hidden_width), "tp", 0, 0, tiled=True
-    )
-    total = jnp.sum(parts.astype(F32), axis=0)
-    hidden = (jax.nn.silu(total[:, :hidden_width]) * total[:, hidden_width:]).astype(BF16)
-    hidden = lax.all_gather(hidden, "tp", axis=0, tiled=True)
+    hidden = exchange(gate_up, n_tp)
     outs = []
     for e in range(experts_local):
         rows = hidden[e * n_sp * cap : (e + 1) * n_sp * cap]

time: 143 us -> 139 us (0.972)
  blocking collectives: 36.5 us -> 13.8 us
  Pallas kernels: 9.76 us -> 27.4 us
    pallas_call x0 -> x1, Pallas kernels: none -> 17.7 us  [exchange(): pl.pallas_call(functools.partial(exchange_kernel, n_tp), out_shape=jax.Sh...]
    all_to_all x1 -> x0, blocking collectives: 16.3 us -> none  [body(): lax.all_to_all(gate_up.reshape(n_tp, rows_all // n_tp, 2 * hidden_width),...]
    all_gather x1 -> x0, blocking collectives: 6.52 us -> none  [body(): hidden = lax.all_gather(hidden, 'tp', axis=0, tiled=True)]
where the time goes in v3:
time: 139 us; the launch traced here: 138 us
  waiting for transfers between devices  50.2 us (36%)
  starting transfers between devices  32 us (23%)
  Pallas kernels  27.4 us (20%)
  blocking collectives  13.8 us (10%)
  matrix products  8.19 us (6%)
  local copies, waits for them, and re-layouts  5.03 us (4%)
  other arithmetic  1.61 us (1%)
    all_to_all x1, starting transfers between devices, body(): lax.all_to_all(send, 'sp', split_axis=0, concat_axis=0, tiled=True)  28.4 us
    all_to_all x1, waiting for transfers between devices, body(): lax.all_to_all(expert_out, 'sp', split_axis=0, concat_axis=0, tiled=True)  26.8 us
    all_to_all x1, waiting for transfers between devices, body(): lax.all_to_all(send, 'sp', split_axis=0, concat_axis=0, tiled=True)  23.4 us
    pallas_call x1, Pallas kernels, exchange(): pl.pallas_call(functools.partial(exchange_kernel, n_tp), out_shape=jax.Sh...  17.7 us
    pallas_call x1, Pallas kernels, attention(): pl.pallas_call(functools.partial(attention_kernel, heads, hd, n_sp, inner...  9.76 us
    all_gather x1, blocking collectives, body(): lax.all_gather(attended, 'tp', axis=1, tiled=True)  7.2 us
    psum x1, blocking collectives, body(): square_sum = lax.psum(jnp.sum(mixed_f * mixed_f, axis=1), 'tp')  6.56 us
    unnamed x27, local copies, waits for them, and re-layouts  4.95 us
  transfers between devices with their start and end apart: 2, of which 2 were waited for; matrix products, arithmetic and copies ran while one was open for 2% of the time, Pallas kernels for 0%

profile of v3, /device:TPU:0, one launch (start us, length us, event | category | flops | bytes accessed | tf_op | source)
XLA Modules:
  0.0 138.4 jit_solution(14961164337410744697)
XLA Ops:
  0.0 0.9 copy.28
  0.9 0.9 copy-done.1
  1.8 0.9 copy-done.2
  2.7 0.9 copy-done.3
  3.6 9.8 %shard_map.145 = bf16[128,512]{1,0:T(8,128)(2,1)S(1)} custom-call(bf16[128,512]{1,0:T(8,128)(2,1)S(1)} %copy-done.1, bf16[128,512]{1,0:T(8,128)(2,1)S(1)} %copy-done.2, bf16[128,512]{1,0:T(8,128)(2,1)S(1)} %copy-done.3, bf16[128,128]{1,0:T(8,128)(2,1)S(1)} %pad.4.b_ref), custom_call_target="tpu_custom_call" | custom-call | flops 2000000000 | bytes 4194304 | tf_op jit(solution)/shard_map/pallas_call | solution.py:184
  13.4 7.2 %all_gather.3 = bf16[128,2048]{1,0:T(8,128)(2,1)S(1)} all-gather(bf16[128,512]{1,0:T(8,128)(2,1)S(1)} %shard_map.145), channel_id=1, replica_groups=mesh['sp'=8,'tp'=4] {'tp'}, dimensions={1}, use_global_device_ids=true | all-gather | bytes 655360 | tf_op jit(solution)/shard_map/all_gather | solution.py:324
  20.6 0.8 fusion.1
  21.4 0.1 fusion.14
  21.5 6.6 %psum.7 = f32[128]{0:T(128)S(1)} all-reduce(f32[128]{0:T(128)S(1)} %fusion.14), channel_id=1, replica_groups=mesh['sp'=8,'tp'=4] {'tp'}, use_global_device_ids=true, to_apply=%region_4.5 | all-reduce | flops 128 | bytes 1024 | tf_op jit(solution)/shard_map/psum | solution.py:329
  28.1 0.1 fusion.22
  28.3 0.1 fusion.17
  28.4 1.5 %convolution_convert_fusion = bf16[512,1024]{1,0:T(8,128)(2,1)} fusion(pred[128,512]{1,0:T(8,128)(4,1)S(1)} %fusion.17, bf16[128,1024]{1,0:T(8,128)(2,1)S(1)} %fusion.1, f32[1024]{0:T(1024)S(1)} %copy-done.7, f32[128]{0:T(128)S(1)} %add_rsqrt_fusion), kind=kOutput, calls=%fused_computation | convolution fusion | flops 135266304 | bytes 1380864 | tf_op jit(solution)/shard_map/dot_general | solution.py:333
  29.9 28.4 %all-to-all-start = ((bf16[8,64,1024]{2,1,0:T(8,128)(2,1)}), bf16[8,64,1024]{2,1,0:T(8,128)(2,1)S(1)}, u32[]{:S(2)}, u32[]{:S(2)}) async-start(bf16[8,64,1024]{2,1,0:T(8,128)(2,1)} %bitcast), calls=%async_computation | async-start | bytes 2097152 | tf_op jit(solution)/shard_map/all_to_all | solution.py:337
  58.3 0.4 convolution_convert_fusion.7
  58.7 1.5 %convolution_convert_fusion.8 = bf16[128,384]{1,0:T(8,128)(2,1)S(1)} fusion(bf16[1024,384]{1,0:T(8,128)(2,1)} %param.27, bf16[128,1024]{1,0:T(8,128)(2,1)S(1)} %fusion.1, f32[1024]{0:T(1024)S(1)} %copy-done.7, f32[128]{0:T(128)S(1)} %add_rsqrt_fusion), kind=kOutput, calls=%fused_computation.13 | convolution fusion | flops 101236736 | bytes 1151488 | tf_op jit(solution)/shard_map/dot_general | solution.py:344
  60.2 23.4 %all-to-all-done = bf16[8,64,1024]{2,1,0:T(8,128)(2,1)S(1)} async-done(((bf16[8,64,1024]{2,1,0:T(8,128)(2,1)}), bf16[8,64,1024]{2,1,0:T(8,128)(2,1)S(1)}, u32[]{:S(2)}, u32[]{:S(2)}) %all-to-all-start) | async-done | bytes 1048608 | tf_op jit(solution)/shard_map/all_to_all | solution.py:337
  83.6 0.1 fusion.27
  83.7 1.3 copy-done.9
  85.0 0.4 convolution_convert_fusion.3
  85.4 0.4 convolution_convert_fusion.4
  85.9 0.4 convolution_convert_fusion.5
  86.3 0.4 convolution_convert_fusion.6
  86.8 0.1 maximum_maximum_fusion
  86.9 17.7 %shard_map.146 = bf16[4,160,384]{2,1,0:T(8,128)(2,1)S(1)} custom-call(bf16[4,160,768]{2,1,0:T(8,128)(2,1)S(1)} %bitcast.45), custom_call_target="tpu_custom_call" | custom-call | flops 100000000 | bytes 2097152 | tf_op jit(solution)/shard_map/pallas_call | solution.py:256
  104.6 0.4 convolution_convert_fusion.1
  105.0 0.4 convolution_convert_fusion.2
  105.5 1.1 pad_maximum_fusion
  106.5 3.6 %all-to-all-start.1 = ((bf16[8,64,1024]{2,1,0:T(8,128)(2,1)}), bf16[8,64,1024]{2,1,0:T(8,128)(2,1)S(1)}, u32[]{:S(2)}, u32[]{:S(2)}) async-start(bf16[8,64,1024]{2,1,0:T(8,128)(2,1)} %bitcast.16), calls=%async_computation.1 | async-start | bytes 2097152 | tf_op jit(solution)/shard_map/all_to_all | solution.py:356
  110.1 0.1 select_reduce_fusion
  110.3 0.3 convolution_add_fusion.2
  110.6 26.8 %all-to-all-done.1 = bf16[8,64,1024]{2,1,0:T(8,128)(2,1)S(1)} async-done(((bf16[8,64,1024]{2,1,0:T(8,128)(2,1)}), bf16[8,64,1024]{2,1,0:T(8,128)(2,1)S(1)}, u32[]{:S(2)}, u32[]{:S(2)}) %all-to-all-start.1) | async-done | bytes 1048608 | tf_op jit(solution)/shard_map/all_to_all | solution.py:356
  137.4 1.0 fusion
  (27 shorter events, 0.1 us)
Async XLA Ops:
  0.0 110.3 %copy-start = (bf16[384,1024]{1,0:T(8,128)(2,1)S(1)}, bf16[384,1024]{1,0:T(8,128)(2,1)}, u32[]{:S(2)}) copy-start(bf16[384,1024]{1,0:T(8,128)(2,1)} %param.29) | copy-start | bytes 2359300
  0.9 0.9 copy-start.1
  1.8 0.9 copy-start.2
  2.7 0.9 copy-start.3
  3.6 17.0 %copy-start.4 = (bf16[2048,1024]{1,0:T(8,128)(2,1)S(1)}, bf16[2048,1024]{1,0:T(8,128)(2,1)}, u32[]{:S(2)}) copy-start(bf16[2048,1024]{1,0:T(8,128)(2,1)} %param.20) | copy-start | bytes 12582916
  3.6 17.0 %copy-start.5 = (bf16[128,1024]{1,0:T(8,128)(2,1)S(1)}, bf16[128,1024]{1,0:T(8,128)(2,1)}, u32[]{:S(2)}) copy-start(bf16[128,1024]{1,0:T(8,128)(2,1)} %param.19) | copy-start | bytes 786436
  20.6 7.5 %copy-start.6 = (s32[128,2]{0,1:T(2,128)S(1)}, s32[128,2]{0,1:T(2,128)}, u32[]{:S(2)}) copy-start(s32[128,2]{0,1:T(2,128)} %param.22) | copy-start | bytes 3076
  20.6 7.8 %copy-start.7 = (f32[1024]{0:T(1024)S(1)}, f32[1024]{0:T(1024)}, u32[]{:S(2)}) copy-start(f32[1024]{0:T(1024)} %param.21) | copy-start | bytes 12292
  21.4 37.0 %copy-start.12 = (bf16[1024,384]{1,0:T(8,128)(2,1)S(1)}, bf16[1024,384]{1,0:T(8,128)(2,1)}, u32[]{:S(2)}) copy-start(bf16[1024,384]{1,0:T(8,128)(2,1)} %param.28) | copy-start | bytes 2359300
  29.9 53.6 %all-to-all-start = ((bf16[8,64,1024]{2,1,0:T(8,128)(2,1)}), bf16[8,64,1024]{2,1,0:T(8,128)(2,1)S(1)}, u32[]{:S(2)}, u32[]{:S(2)}) async-start(bf16[8,64,1024]{2,1,0:T(8,128)(2,1)} %bitcast), calls=%async_computation | async-start | bytes 2097152 | tf_op jit(solution)/shard_map/all_to_all | solution.py:337
  83.6 1.4 %copy-start.9 = (bf16[2,1024,384]{2,1,0:T(8,128)(2,1)S(1)}, bf16[2,1024,384]{2,1,0:T(8,128)(2,1)}, u32[]{:S(2)}) copy-start(bf16[2,1024,384]{2,1,0:T(8,128)(2,1)} %param.25) | copy-start | bytes 4718596
  83.7 2.2 %copy-start.10 = (bf16[2,1024,384]{2,1,0:T(8,128)(2,1)S(1)}, bf16[2,1024,384]{2,1,0:T(8,128)(2,1)}, u32[]{:S(2)}) copy-start(bf16[2,1024,384]{2,1,0:T(8,128)(2,1)} %param.24) | copy-start | bytes 4718596
  86.8 17.8 %copy-start.11 = (bf16[2,384,1024]{2,1,0:T(8,128)(2,1)S(1)}, bf16[2,384,1024]{2,1,0:T(8,128)(2,1)}, u32[]{:S(2)}) copy-start(bf16[2,384,1024]{2,1,0:T(8,128)(2,1)} %param.26) | copy-start | bytes 4718596
  105.5 4.7 %copy-start.8 = (f32[128,2]{0,1:T(2,128)S(1)}, f32[128,2]{0,1:T(2,128)}, u32[]{:S(2)}) copy-start(f32[128,2]{0,1:T(2,128)} %param.23) | copy-start | bytes 3076
  106.5 30.9 %all-to-all-start.1 = ((bf16[8,64,1024]{2,1,0:T(8,128)(2,1)}), bf16[8,64,1024]{2,1,0:T(8,128)(2,1)S(1)}, u32[]{:S(2)}, u32[]{:S(2)}) async-start(bf16[8,64,1024]{2,1,0:T(8,128)(2,1)} %bitcast.16), calls=%async_computation.1 | async-start | bytes 2097152 | tf_op jit(solution)/shard_map/all_to_all | solution.py:356
